TPU v7x, 128 devices: a whole 4x4x4 slice. The times are simulated.
128 devices in a mesh: sp: 64 (over z, y, x), tp: 2 (over core).
Axes of the slice: x: 4, y: 4, z: 4, core: 2. Of those that a mesh axis runs over, the one named last changes fastest.
Arguments:
- cotangent: bfloat16 [12288, 2048], P('sp'), may hold values from -1.75 to 1.75
- mixed_input: bfloat16 [12288, 2048], P('sp'), may hold values from -6 to 6
- route_ids: int32 [12288, 2], P('sp'), may hold values from 0 to 63, all different within a row; in each aligned block of 192 rows (0 to 191, 192 to 383, ...) at most 12 rows name the same one
- route_gates: float32 [12288, 2], P('sp'), may hold values from 0.25 to 1.5
- expert_gate: bfloat16 [64, 2048, 1024], P('sp', None, 'tp'), may hold values from -0.125 to 0.125
- expert_up: bfloat16 [64, 2048, 1024], P('sp', None, 'tp'), may hold values from -0.125 to 0.125
- expert_down: bfloat16 [64, 1024, 2048], P('sp', 'tp'), may hold values from -0.1875 to 0.1875
- projection: bfloat16 [2048, 1024], P(None, 'tp'), may hold values from -0.1875 to 0.1875
- mixer_output: bfloat16 [12288, 1024], P('sp', 'tp'), may hold values from -6 to 6
- query_rows: bfloat16 [12288, 512], P('sp', 'tp'), may hold values from -6 to 6
- key_rows: bfloat16 [12288, 512], P('sp', 'tp'), may hold values from -0.75 to 0.75
- value_rows: bfloat16 [12288, 1024], P('sp', 'tp'), may hold values from -6 to 6
- log_forward: float32 [12288, 512], P('sp', 'tp'), may hold values from -0.25 to 0, as said below
- log_backward: float32 [12288, 512], P('sp', 'tp'), may hold values from -0.25 to 0, as said below
Outputs:
- gate_grad: float32 [64, 2048, 1024], P('sp', None, 'tp')
- up_grad: float32 [64, 2048, 1024], P('sp', None, 'tp')
- down_grad: float32 [64, 1024, 2048], P('sp', 'tp')
- projection_grad: float32 [2048, 1024], P('sp', 'tp')
- query_grad: float32 [12288, 512], P('sp', 'tp')
- key_grad: float32 [12288, 512], P('sp', 'tp')
- value_grad: float32 [12288, 1024], P('sp', 'tp')
- log_forward_grad: float32 [12288, 512], P('sp', 'tp')
- log_backward_grad: float32 [12288, 512], P('sp', 'tp')
Inputs may be any that keep to these rules, and one draw needn't show every extreme that they name: `route_ids`: in the rows of one device no expert is named by more than 12 routes, a bound that some block reaches in the rows of some device; the 2 experts of a token differ. `log_forward`: strictly negative. `log_backward`: strictly negative.
All inputs are finite; a program needn't handle non-finite values.
Results may differ from a plain program's by a relative error of at most 0.006.
Values may be sent and summed in bfloat16 or wider, within the bound.
A program may use at most 192 MiB of HBM per device.

v0:
```python
import jax
import jax.numpy as jnp
from jax import lax
from jax.sharding import Mesh
from jax.sharding import PartitionSpec as P

DK = 32
DV = 64
BLK = 64
SP = ("sp_0", "sp_1", "sp_2")


topmost_precision = lax.Precision.HIGHEST


def neutral_like(x, identity):
    return jax.tree.map(
        lambda a, e: jnp.broadcast_to(jnp.asarray(e, a.dtype), a.shape), x, identity
    )


def prefix_by_axis(x, axes, combine, identity, reverse):
    before = start = neutral_like(x, identity)
    so_far = x
    for axis in reversed(axes):
        count, place = (lax.axis_size(axis), lax.axis_index(axis))
        pieces = jax.tree.map(lambda part: lax.all_gather(part, axis), so_far)
        inside, so_far = (start, start)
        for k in reversed(range(count)) if reverse else range(count):
            passed = k > place if reverse else k < place
            so_far = combine(so_far, jax.tree.map(lambda part: part[k], pieces))
            inside = jax.tree.map(lambda new, old: jnp.where(passed, new, old), so_far, inside)
        before = combine(inside, before)
    return before


def sent_together(arrays, axis, split_dim, concat_dim, along):
    widths = [a.shape[along] for a in arrays]
    both = jnp.concatenate(arrays, axis=along)
    whole = lax.all_to_all(both, axis, split_axis=split_dim, concat_axis=concat_dim, tiled=True)
    return tuple(jnp.split(whole, [sum(widths[:k]) for k in range(1, len(widths))], axis=along))


def from_everyone(x, axis):
    count = lax.axis_size(axis)
    return lax.all_to_all(jnp.broadcast_to(x[None], (count, *x.shape)), axis, 0, 0, tiled=True)


def of_everyone(x, axis):
    return from_everyone(x, axis).astype(jnp.float32).sum(axis=0)


def split_up(x, dim, count):
    lengths = x.shape
    tiles = x.reshape(*lengths[:dim], count, lengths[dim] // count, *lengths[dim + 1 :])
    return jnp.moveaxis(tiles, dim, 0)


def summed_on_arrival(x, axis, dim):
    count = lax.axis_size(axis)
    tiles = lax.all_to_all(split_up(x, dim, count), axis, 0, 0, tiled=True)
    return jnp.sum(tiles, axis=0)


def decayed_pass(query_stack, key_matrix, value_matrix, log_rate, entering):
    count = query_stack.shape[0]
    head_count = query_stack.shape[1]
    key_width = query_stack.shape[2]
    value_width = value_matrix.shape[2]
    blocks = count // BLK
    query_blocks = query_stack.reshape(blocks, BLK, head_count, key_width)
    key_blocks = key_matrix.reshape(blocks, BLK, head_count, key_width)
    value_blocks = value_matrix.reshape(blocks, BLK, head_count, value_width)
    running_prefix = jnp.cumsum(log_rate.reshape(blocks, BLK, head_count, key_width), axis=1)
    last_cum = running_prefix[:, -1:]
    increment = jnp.einsum(
        "nlhk,nlhv->nhkv",
        key_blocks * jnp.exp(last_cum - running_prefix),
        value_blocks,
        precision=topmost_precision,
    )
    decay = jnp.exp(last_cum[:, 0])

    def advance(carried, inputs):
        factor, added = inputs
        return (factor[..., None] * carried + added, carried)

    final_state, entering_states = lax.scan(advance, entering, (decay, increment))
    inter_part = jnp.einsum(
        "nlhk,nhkv->nlhv",
        query_blocks * jnp.exp(running_prefix),
        entering_states,
        precision=topmost_precision,
    )
    middle = running_prefix[:, BLK // 2 - 1 : BLK // 2]
    scores = jnp.einsum(
        "nlhk,nmhk->nhlm",
        query_blocks * jnp.exp(running_prefix - middle),
        key_blocks * jnp.exp(middle - running_prefix),
        precision=topmost_precision,
    )
    lower_mask = jnp.tril(jnp.ones((BLK, BLK), bool))
    scores = jnp.where(lower_mask, scores, jnp.float32(0.0))
    intra_part = jnp.einsum("nhlm,nmhv->nlhv", scores, value_blocks, precision=topmost_precision)
    return ((inter_part + intra_part).reshape(count, head_count, value_width), final_state)


def reverse_rows(source_array):
    return jnp.flip(source_array, axis=0)


def span_summary(key_matrix, value_matrix, log_rate):
    running_prefix = jnp.cumsum(log_rate, axis=0)
    summed_values = running_prefix[-1]
    carried = jnp.einsum(
        "zly,zlq->lyq",
        key_matrix * jnp.exp(summed_values[None] - running_prefix),
        value_matrix,
        precision=topmost_precision,
    )
    return (jnp.exp(summed_values), carried, running_prefix)


def combine_maps(earlier, later):
    return tuple(
        (
            (
                earlier_pair[0] * later_pair[0],
                later_pair[0][..., None] * earlier_pair[1] + later_pair[1],
            )
            for earlier_pair, later_pair in zip(earlier, later)
        )
    )


def mixer_grads(query_rows, key_rows, value_rows, log_forward, log_backward, mix_grad):
    tok_count = query_rows.shape[0]
    head_count = query_rows.shape[1] // DK
    query_scaling = DK ** (-0.5)

    def by_heads(source_array, head_width):
        return source_array.astype(jnp.float32).reshape(tok_count, head_count, head_width)

    query_stack = by_heads(query_rows, DK)
    key_matrix = by_heads(key_rows, DK)
    value_matrix = by_heads(value_rows, DV)
    rate_fwd = by_heads(log_forward, DK)
    rate_bwd = by_heads(log_backward, DK)
    output_gradient = by_heads(mix_grad, DV)
    decay_fwd, carried_fwd, forward_running_total = span_summary(key_matrix, value_matrix, rate_fwd)
    decay_bwd, carried_bwd, cumul_bwd = span_summary(
        reverse_rows(key_matrix), reverse_rows(value_matrix), reverse_rows(rate_bwd)
    )
    pulled_fwd = jnp.einsum(
        "zly,zlq->lyq",
        query_stack * query_scaling * jnp.exp(forward_running_total),
        output_gradient,
        precision=topmost_precision,
    )
    pulled_bwd = jnp.einsum(
        "zly,zlq->lyq",
        reverse_rows(query_stack) * query_scaling * jnp.exp(cumul_bwd),
        reverse_rows(output_gradient),
        precision=topmost_precision,
    )
    unit_decay = jnp.ones_like(decay_fwd)
    empty_state = jnp.zeros_like(carried_fwd)
    identity_maps = ((unit_decay, empty_state), (unit_decay, empty_state))
    lower_maps = prefix_by_axis(
        ((decay_fwd, carried_fwd), (decay_bwd, pulled_bwd)), SP, combine_maps, identity_maps, False
    )
    upper_maps = prefix_by_axis(
        ((decay_bwd, carried_bwd), (decay_fwd, pulled_fwd)), SP, combine_maps, identity_maps, True
    )
    state_fwd = lower_maps[0][1]
    leave_bwd_grad = lower_maps[1][1]
    state_bwd = upper_maps[0][1]
    leave_fwd_grad = upper_maps[1][1]

    def local_mixer(query_in, key_in, value_in, forward_in, backward_in):
        out_fwd, leave_fwd = decayed_pass(
            query_in * query_scaling, key_in, value_in, forward_in, state_fwd
        )
        out_bwd, leave_bwd = decayed_pass(
            reverse_rows(query_in) * query_scaling,
            reverse_rows(key_in),
            reverse_rows(value_in),
            reverse_rows(backward_in),
            state_bwd,
        )
        return (out_fwd + reverse_rows(out_bwd), leave_fwd, leave_bwd)

    _, pullback = jax.vjp(local_mixer, query_stack, key_matrix, value_matrix, rate_fwd, rate_bwd)
    grads = pullback((output_gradient, leave_fwd_grad, leave_bwd_grad))
    return tuple((gradient.reshape(tok_count, -1) for gradient in grads))


def local(
    cotangent,
    mixed_input,
    route_ids,
    route_gates,
    expert_gate,
    expert_up,
    expert_down,
    projection,
    mixer_output,
    query_rows,
    key_rows,
    value_rows,
    log_forward,
    log_backward,
):
    tok_count = cotangent.shape[0]
    feature_count = cotangent.shape[1]
    groups = lax.axis_size(SP)
    slot_count = 4 * tok_count // groups
    route_count = route_ids.shape[1]
    flat_ids = route_ids.reshape(-1)
    assigned = flat_ids.shape[0]
    onehot = (flat_ids[:, None] == jnp.arange(groups, dtype=jnp.int32)[None, :]).astype(jnp.int32)
    rank = jnp.sum((jnp.cumsum(onehot, axis=0) - 1) * onehot, axis=1)
    destination = flat_ids * slot_count + rank
    source = (
        jnp.full((groups * slot_count,), assigned, jnp.int32)
        .at[destination]
        .set(jnp.arange(assigned, dtype=jnp.int32))
    )
    token_of = source // route_count
    gate_padded = jnp.concatenate([route_gates.reshape(-1), jnp.zeros((1,), jnp.float32)])
    cot_padded = jnp.concatenate([cotangent, jnp.zeros((1, feature_count), jnp.bfloat16)], axis=0)
    input_padded = jnp.concatenate(
        [mixed_input, jnp.zeros((1, feature_count), jnp.bfloat16)], axis=0
    )
    routed_cot = (
        (gate_padded[source][:, None] * cot_padded[token_of].astype(jnp.float32))
        .astype(jnp.bfloat16)
        .reshape(groups, slot_count, feature_count)
    )
    routed_tok = input_padded[token_of].reshape(groups, slot_count, feature_count)
    w_gate = expert_gate[0]
    w_up = expert_up[0]
    w_down = expert_down[0]
    contract_last = (((1,), (1,)), ((), ()))
    contract_first = (((0,), (0,)), ((), ()))
    cot_in, tok_in = sent_together((routed_cot, routed_tok), SP, 0, 0, 1)
    row_total = cot_in.shape[0] * cot_in.shape[1]
    cot_block = cot_in.reshape(row_total, feature_count)
    tok_block = tok_in.reshape(row_total, feature_count)
    gate_pre = jnp.dot(tok_block, w_gate, preferred_element_type=jnp.float32)
    up_pre = jnp.dot(tok_block, w_up, preferred_element_type=jnp.float32)
    sigmoid_gate = jax.nn.sigmoid(gate_pre)
    silu_gate = gate_pre * sigmoid_gate
    hidden = (silu_gate * up_pre).astype(jnp.bfloat16)
    hidden_grad = lax.dot_general(
        cot_block, w_down, contract_last, preferred_element_type=jnp.float32
    )
    slope = sigmoid_gate * (1.0 + gate_pre * (1.0 - sigmoid_gate))
    gate_pre_grad = (hidden_grad * up_pre * slope).astype(jnp.bfloat16)
    up_pre_grad = (hidden_grad * silu_gate).astype(jnp.bfloat16)
    partial_value = lax.dot_general(
        gate_pre_grad, w_gate, contract_last, preferred_element_type=jnp.float32
    )
    partial_value = partial_value + lax.dot_general(
        up_pre_grad, w_up, contract_last, preferred_element_type=jnp.float32
    )
    down_term = lax.dot_general(
        hidden, cot_block, contract_first, preferred_element_type=jnp.float32
    )
    gate_term = lax.dot_general(
        tok_block, gate_pre_grad, contract_first, preferred_element_type=jnp.float32
    )
    up_term = lax.dot_general(
        tok_block, up_pre_grad, contract_first, preferred_element_type=jnp.float32
    )
    summed = (
        of_everyone(partial_value.astype(jnp.bfloat16), "tp")
        .astype(jnp.float32)
        .astype(jnp.bfloat16)
    )
    returned = lax.all_to_all(
        summed.reshape(cot_in.shape[0], cot_in.shape[1], summed.shape[1]),
        SP,
        split_axis=0,
        concat_axis=0,
        tiled=True,
    )
    expert_terms = (gate_term, up_term, down_term)
    column_count = returned.shape[2]
    per_route = returned.reshape(groups * slot_count, column_count)[destination].reshape(
        tok_count, route_count, column_count
    )
    mid_grad = (
        jnp.sum(per_route.astype(jnp.float32), axis=1) + cotangent.astype(jnp.float32)
    ).astype(jnp.bfloat16)
    mix_grad = jnp.dot(mid_grad, projection, preferred_element_type=jnp.float32).astype(
        jnp.bfloat16
    )
    projection_grad = summed_on_arrival(
        lax.dot_general(mid_grad, mixer_output, contract_first, preferred_element_type=jnp.float32),
        SP,
        0,
    )
    query_grad, key_grad, value_grad, log_forward_grad, log_backward_grad = mixer_grads(
        query_rows, key_rows, value_rows, log_forward, log_backward, mix_grad
    )
    return (
        expert_terms[0][None],
        expert_terms[1][None],
        expert_terms[2][None],
        projection_grad,
        query_grad,
        key_grad,
        value_grad,
        log_forward_grad,
        log_backward_grad,
    )


def solution(mesh):
    finer = Mesh(mesh.devices.reshape(4, 4, 4, mesh.shape["tp"]), ("sp_0", "sp_1", "sp_2", "tp"))
    return jax.shard_map(
        local,
        mesh=finer,
        in_specs=(
            P(SP, None),
            P(SP, None),
            P(SP, None),
            P(SP, None),
            P(SP, None, "tp"),
            P(SP, None, "tp"),
            P(SP, "tp", None),
            P(None, "tp"),
            P(SP, "tp"),
            P(SP, "tp"),
            P(SP, "tp"),
            P(SP, "tp"),
            P(SP, "tp"),
            P(SP, "tp"),
        ),
        out_specs=(
            P(SP, None, "tp"),
            P(SP, None, "tp"),
            P(SP, "tp", None),
            P(SP, "tp"),
            P(SP, "tp"),
            P(SP, "tp"),
            P(SP, "tp"),
            P(SP, "tp"),
            P(SP, "tp"),
        ),
        check_vma=False,
    )
```

profile of v0, /device:TPU:0, one launch (start us, length us, event | category | flops | bytes accessed | tf_op | source)
XLA Modules:
  0.0 739.0 jit_solution(17714213345103939980)
XLA Ops:
  41.9 8.9 %pad_maximum_fusion = bf16[64,24,2048]{2,1,0:T(8,128)(2,1)} fusion(bf16[64,12,2048]{2,1,0:T(8,128)(2,1)} %reshape.576, bf16[64,12,2048]{2,1,0:T(8,128)(2,1)} %multiply_convert_fusion), kind=kLoop, calls=%fused_computation.26 | loop fusion | flops 12582912 | bytes 12582912 | tf_op jit(solution)/shard_map/concatenate | solution.py:39
  50.8 12.4 %all-to-all-start = ((bf16[64,24,2048]{2,1,0:T(8,128)(2,1)}), bf16[64,24,2048]{2,1,0:T(8,128)(2,1)}, u32[]{:S(2)}, u32[]{:S(2)}) async-start(bf16[64,24,2048]{2,1,0:T(8,128)(2,1)} %pad_maximum_fusion), calls=%async_computation | async-start | bytes 12582912 | tf_op jit(solution)/shard_map/all_to_all | solution.py:40
  63.9 18.0 %reduce-window.24 = f32[32,8,2,128]{3,1,2,0:T(8,128)S(1)} reduce-window(f32[32,8,2,128]{3,1,2,0:T(8,128)S(1)} %pad_bitcast_fusion.1, f32[]{:T(128)} %constant.194.clone.1), window={size=1x1x1x128 pad=0_0x0_0x0_0x127_0}, to_apply=%region_8.9 | reduce-window | flops 8323072 | bytes 524292 | tf_op jit(solution)/shard_map/reduce-window.2
  82.8 18.0 %reduce-window.26 = f32[32,8,2,128]{3,1,2,0:T(8,128)S(1)} reduce-window(f32[32,8,2,128]{3,1,2,0:T(8,128)S(1)} %pad_bitcast_fusion, f32[]{:T(128)} %constant.194.clone.1), window={size=1x1x1x128 pad=0_0x0_0x0_0x127_0}, to_apply=%region_13.14 | reduce-window | flops 8323072 | bytes 524292 | tf_op jit(solution)/shard_map/reduce-window.4
  142.5 12.5 %all_gather.100 = f32[4,8,32]{2,1,0:T(8,128)S(1)} all-gather(f32[1,8,32]{2,1,0:T(8,128)S(1)} %get-tuple-element.714), channel_id=1, replica_groups=mesh['sp_0'=4,'sp_1'=4,'sp_2'=4,'tp'=2] {'sp_2'}, dimensions={0}, use_global_device_ids=true | all-gather | bytes 5120 | tf_op jit(solution)/shard_map/all_gather | solution.py:27
  155.7 12.3 %all_gather.114 = f32[4,8,32]{2,1,0:T(8,128)S(1)} all-gather(f32[1,8,32]{2,1,0:T(8,128)S(1)} %get-tuple-element.679), channel_id=1, replica_groups=mesh['sp_0'=4,'sp_1'=4,'sp_2'=4,'tp'=2] {'sp_1'}, dimensions={0}, use_global_device_ids=true | all-gather | bytes 5120 | tf_op jit(solution)/shard_map/all_gather | solution.py:27
  168.0 12.0 %all_gather.101 = f32[4,8,32]{2,1,0:T(8,128)S(1)} all-gather(f32[1,8,32]{2,1,0:T(8,128)S(1)} %get-tuple-element.681), channel_id=1, replica_groups=mesh['sp_0'=4,'sp_1'=4,'sp_2'=4,'tp'=2] {'sp_1'}, dimensions={0}, use_global_device_ids=true | all-gather | bytes 5120 | tf_op jit(solution)/shard_map/all_gather | solution.py:27
  180.6 12.5 %all_gather.102 = f32[4,8,32]{2,1,0:T(8,128)S(1)} all-gather(f32[1,8,32]{2,1,0:T(8,128)S(1)} %get-tuple-element.689), channel_id=1, replica_groups=mesh['sp_0'=4,'sp_1'=4,'sp_2'=4,'tp'=2] {'sp_0'}, dimensions={0}, use_global_device_ids=true | all-gather | bytes 5120 | tf_op jit(solution)/shard_map/all_gather | solution.py:27
  193.6 12.0 %all_gather.115 = f32[4,8,32]{2,1,0:T(8,128)S(1)} all-gather(f32[1,8,32]{2,1,0:T(8,128)S(1)} %get-tuple-element.672), channel_id=1, replica_groups=mesh['sp_0'=4,'sp_1'=4,'sp_2'=4,'tp'=2] {'sp_0'}, dimensions={0}, use_global_device_ids=true | all-gather | bytes 5120 | tf_op jit(solution)/shard_map/all_gather | solution.py:27
  205.6 12.0 %all_gather.107 = f32[4,8,32]{2,1,0:T(8,128)S(1)} all-gather(f32[1,8,32]{2,1,0:T(8,128)S(1)} %get-tuple-element.644), channel_id=1, replica_groups=mesh['sp_0'=4,'sp_1'=4,'sp_2'=4,'tp'=2] {'sp_2'}, dimensions={0}, use_global_device_ids=true | all-gather | bytes 5120 | tf_op jit(solution)/shard_map/all_gather | solution.py:27
  218.3 12.0 %all_gather.120 = f32[4,8,32]{2,1,0:T(8,128)S(1)} all-gather(f32[1,8,32]{2,1,0:T(8,128)S(1)} %get-tuple-element.662), channel_id=1, replica_groups=mesh['sp_0'=4,'sp_1'=4,'sp_2'=4,'tp'=2] {'sp_1'}, dimensions={0}, use_global_device_ids=true | all-gather | bytes 5120 | tf_op jit(solution)/shard_map/all_gather | solution.py:27
  230.3 12.0 %all_gather.108 = f32[4,8,32]{2,1,0:T(8,128)S(1)} all-gather(f32[1,8,32]{2,1,0:T(8,128)S(1)} %get-tuple-element.664), channel_id=1, replica_groups=mesh['sp_0'=4,'sp_1'=4,'sp_2'=4,'tp'=2] {'sp_1'}, dimensions={0}, use_global_device_ids=true | all-gather | bytes 5120 | tf_op jit(solution)/shard_map/all_gather | solution.py:27
  242.9 12.0 %all_gather.109 = f32[4,8,32]{2,1,0:T(8,128)S(1)} all-gather(f32[1,8,32]{2,1,0:T(8,128)S(1)} %get-tuple-element.698), channel_id=1, replica_groups=mesh['sp_0'=4,'sp_1'=4,'sp_2'=4,'tp'=2] {'sp_0'}, dimensions={0}, use_global_device_ids=true | all-gather | bytes 5120 | tf_op jit(solution)/shard_map/all_gather | solution.py:27
  255.5 12.5 %all_gather.121 = f32[4,8,32]{2,1,0:T(8,128)} all-gather(f32[1,8,32]{2,1,0:T(8,128)S(1)} %get-tuple-element.655), channel_id=1, replica_groups=mesh['sp_0'=4,'sp_1'=4,'sp_2'=4,'tp'=2] {'sp_0'}, dimensions={0}, use_global_device_ids=true | all-gather | bytes 5120 | tf_op jit(solution)/shard_map/all_gather | solution.py:27
  270.8 13.5 %all-gather = f32[32,32,64]{2,1,0:T(8,128)} all-gather(f32[8,32,64]{2,1,0:T(8,128)S(1)} %fusion.20), channel_id=2, replica_groups=mesh['sp_0'=4,'sp_1'=4,'sp_2'=4,'tp'=2] {'sp_2'}, dimensions={0}, use_global_device_ids=true | all-gather | bytes 327680 | tf_op jit(solution)/shard_map/all_gather | solution.py:27
  286.2 13.7 %all-gather.1 = f32[32,32,64]{2,1,0:T(8,128)} all-gather(f32[8,32,64]{2,1,0:T(8,128)S(1)} %fusion.18), channel_id=3, replica_groups=mesh['sp_0'=4,'sp_1'=4,'sp_2'=4,'tp'=2] {'sp_2'}, dimensions={0}, use_global_device_ids=true | all-gather | bytes 327680 | tf_op jit(solution)/shard_map/all_gather | solution.py:27
  345.9 10.0 %all_to_all.20 = bf16[2,768,2048]{2,1,0:T(8,128)(2,1)} all-to-all(bf16[2,768,2048]{2,1,0:T(8,128)(2,1)S(1)} %broadcast_in_dim.130), channel_id=1, replica_groups=mesh['sp_0'=4,'sp_1'=4,'sp_2'=4,'tp'=2] {'tp'}, dimensions={0} | all-to-all | bytes 12582912 | tf_op jit(solution)/shard_map/all_to_all | solution.py:46
  368.9 9.1 %all-to-all-start.2 = ((bf16[64,12,2048]{2,1,0:T(8,128)(2,1)}), bf16[64,12,2048]{2,1,0:T(8,128)(2,1)}, u32[]{:S(2)}, u32[]{:S(2)}) async-start(bf16[64,12,2048]{2,1,0:T(8,128)(2,1)} %reshape.579), calls=%async_computation.2 | async-start | bytes 8388608 | tf_op jit(solution)/shard_map/all_to_all | solution.py:281
  399.3 33.0 %all-to-all-done.2 = bf16[64,12,2048]{2,1,0:T(8,128)(2,1)} async-done(((bf16[64,12,2048]{2,1,0:T(8,128)(2,1)}), bf16[64,12,2048]{2,1,0:T(8,128)(2,1)}, u32[]{:S(2)}, u32[]{:S(2)}) %all-to-all-start.2) | async-done | bytes 3145760 | tf_op jit(solution)/shard_map/all_to_all | solution.py:281
  467.0 13.4 %all-gather.2 = f32[32,32,64]{2,1,0:T(8,128)S(1)} all-gather(f32[8,32,64]{2,1,0:T(8,128)S(1)} %fusion.16), channel_id=4, replica_groups=mesh['sp_0'=4,'sp_1'=4,'sp_2'=4,'tp'=2] {'sp_2'}, dimensions={0}, use_global_device_ids=true | all-gather | bytes 327680 | tf_op jit(solution)/shard_map/all_gather | solution.py:27
  481.3 12.8 %all_gather.105 = f32[4,8,32,64]{3,2,1,0:T(8,128)S(1)} all-gather(f32[1,8,32,64]{3,2,1,0:T(8,128)S(1)} %get-tuple-element.706), channel_id=1, replica_groups=mesh['sp_0'=4,'sp_1'=4,'sp_2'=4,'tp'=2] {'sp_1'}, dimensions={0}, use_global_device_ids=true | all-gather | bytes 327680 | tf_op jit(solution)/shard_map/all_gather | solution.py:27
  494.4 13.1 %all_gather.106 = f32[4,8,32,64]{3,2,1,0:T(8,128)S(1)} all-gather(f32[1,8,32,64]{3,2,1,0:T(8,128)S(1)} %multiply_add_fusion.6), channel_id=1, replica_groups=mesh['sp_0'=4,'sp_1'=4,'sp_2'=4,'tp'=2] {'sp_0'}, dimensions={0}, use_global_device_ids=true | all-gather | bytes 327680 | tf_op jit(solution)/shard_map/all_gather | solution.py:27
  508.8 9.0 %while.64 = (s32[]{:T(128)}, f32[8,32,64]{2,1,0:T(8,128)S(1)}, f32[3,8,32,64]{3,2,1,0:T(8,128)S(1)}, f32[3,8,32,1]{2,1,3,0:T(8,128)}, f32[3,8,32]{2,1,0:T(8,128)}, /*index=5*/f32[3,8,32,64]{3,2,1,0:T(8,128)}, s32[]{:T(128)}) while((s32[]{:T(128)}, f32[8,32,64]{2,1,0:T(8,128)S(1)}, f32[3,8,32,64]{3,2,1,0:T(8,128)S(1)}, ...), condition=%wide.region_11.12_spmd, body=%wide.region_10.11_spmd.sunk | while | flops 32770 | bytes 470617 | solution.py:88
  517.8 13.0 %all_gather.118 = f32[4,8,32,64]{3,2,1,0:T(8,128)S(1)} all-gather(f32[1,8,32,64]{3,2,1,0:T(8,128)} %get-tuple-element.705), channel_id=1, replica_groups=mesh['sp_0'=4,'sp_1'=4,'sp_2'=4,'tp'=2] {'sp_1'}, dimensions={0}, use_global_device_ids=true | all-gather | bytes 327680 | tf_op jit(solution)/shard_map/all_gather | solution.py:27
  531.7 13.0 %all_gather.119 = f32[4,8,32,64]{3,2,1,0:T(8,128)S(1)} all-gather(f32[1,8,32,64]{3,2,1,0:T(8,128)S(1)} %multiply_add_fusion.4), channel_id=1, replica_groups=mesh['sp_0'=4,'sp_1'=4,'sp_2'=4,'tp'=2] {'sp_0'}, dimensions={0}, use_global_device_ids=true | all-gather | bytes 327680 | tf_op jit(solution)/shard_map/all_gather | solution.py:27
  547.8 9.2 %while.66 = (s32[]{:T(128)}, f32[8,32,64]{2,1,0:T(8,128)S(1)}, f32[3,8,32]{2,1,0:T(8,128)}, f32[3,8,32,64]{3,2,1,0:T(8,128)}, f32[3,8,32,64]{3,2,1,0:T(8,128)}, ...) while((s32[]{:T(128)}, f32[8,32,64]{2,1,0:T(8,128)S(1)}, ...), condition=%wide.region_19.20_spmd, body=%wide.region_17.19_spmd.sunk | while | flops 65283 | bytes 468089 | solution.py:88
  569.0 12.8 %all-gather.3 = f32[32,32,64]{2,1,0:T(8,128)S(1)} all-gather(f32[8,32,64]{2,1,0:T(8,128)S(1)} %fusion.14), channel_id=5, replica_groups=mesh['sp_0'=4,'sp_1'=4,'sp_2'=4,'tp'=2] {'sp_2'}, dimensions={0}, use_global_device_ids=true | all-gather | bytes 327680 | tf_op jit(solution)/shard_map/all_gather | solution.py:27
  582.1 12.8 %all_gather.112 = f32[4,8,32,64]{3,2,1,0:T(8,128)S(1)} all-gather(f32[1,8,32,64]{3,2,1,0:T(8,128)S(1)} %get-tuple-element.704), channel_id=1, replica_groups=mesh['sp_0'=4,'sp_1'=4,'sp_2'=4,'tp'=2] {'sp_1'}, dimensions={0}, use_global_device_ids=true | all-gather | bytes 327680 | tf_op jit(solution)/shard_map/all_gather | solution.py:27
  595.2 12.8 %all_gather.113 = f32[4,8,32,64]{3,2,1,0:T(8,128)S(1)} all-gather(f32[1,8,32,64]{3,2,1,0:T(8,128)S(1)} %multiply_add_fusion.5), channel_id=1, replica_groups=mesh['sp_0'=4,'sp_1'=4,'sp_2'=4,'tp'=2] {'sp_0'}, dimensions={0}, use_global_device_ids=true | all-gather | bytes 327680 | tf_op jit(solution)/shard_map/all_gather | solution.py:27
  614.7 12.8 %all_gather.124 = f32[4,8,32,64]{3,2,1,0:T(8,128)S(1)} all-gather(f32[1,8,32,64]{3,2,1,0:T(8,128)S(1)} %get-tuple-element.703), channel_id=1, replica_groups=mesh['sp_0'=4,'sp_1'=4,'sp_2'=4,'tp'=2] {'sp_1'}, dimensions={0}, use_global_device_ids=true | all-gather | bytes 327680 | tf_op jit(solution)/shard_map/all_gather | solution.py:27
  628.5 13.5 %all_gather.125 = f32[4,8,32,64]{3,2,1,0:T(8,128)} all-gather(f32[1,8,32,64]{3,2,1,0:T(8,128)S(1)} %multiply_add_fusion.3), channel_id=1, replica_groups=mesh['sp_0'=4,'sp_1'=4,'sp_2'=4,'tp'=2] {'sp_0'}, dimensions={0}, use_global_device_ids=true | all-gather | bytes 327680 | tf_op jit(solution)/shard_map/all_gather | solution.py:27
  708.8 19.4 %fusion.161 = f32[3,64,8,32]{3,2,1,0:T(8,128)S(1)} fusion(f32[3,64,8,32]{3,2,1,0:T(8,128)S(1)} %copy.1973), kind=kOutput, calls=%fused_computation.376 | output fusion | flops 3096576 | bytes 393216 | tf_op jit(solution)/shard_map/transpose(jvp(jit(cumsum)))/reduce_window_sum | solution.py:74
  (469 shorter events, 339.3 us)
Async XLA Ops:
  0.6 320.5 %copy-start = (bf16[1,2048,512]{2,1,0:T(8,128)(2,1)S(1)}, bf16[1,2048,512]{2,1,0:T(8,128)(2,1)}, u32[]{:S(2)}) copy-start(bf16[1,2048,512]{2,1,0:T(8,128)(2,1)} %param.26) | copy-start | bytes 6291460
  50.8 257.5 %all-to-all-start = ((bf16[64,24,2048]{2,1,0:T(8,128)(2,1)}), bf16[64,24,2048]{2,1,0:T(8,128)(2,1)}, u32[]{:S(2)}, u32[]{:S(2)}) async-start(bf16[64,24,2048]{2,1,0:T(8,128)(2,1)} %pad_maximum_fusion), calls=%async_computation | async-start | bytes 12582912 | tf_op jit(solution)/shard_map/all_to_all | solution.py:40
  123.1 259.3 %copy-start.2 = (f32[3,64,8,32]{1,3,2,0:T(8,128)}, f32[3,64,8,32]{1,3,2,0:T(8,128)S(1)}, u32[]{:S(2)}) copy-start(f32[3,64,8,32]{1,3,2,0:T(8,128)S(1)} %copy.1903) | copy-start | bytes 589828
  125.5 256.9 %copy-start.4 = (f32[3,64,8,32]{1,3,2,0:T(8,128)}, f32[3,64,8,32]{1,3,2,0:T(8,128)S(1)}, u32[]{:S(2)}) copy-start(f32[3,64,8,32]{1,3,2,0:T(8,128)S(1)} %copy.1904) | copy-start | bytes 589828
  135.3 148.9 %copy-start.36 = (bf16[192,512]{0,1:T(8,128)(2,1)S(1)}, bf16[192,512]{0,1:T(8,128)(2,1)}, u32[]{:S(2)}) copy-start(bf16[192,512]{0,1:T(8,128)(2,1)} %copy-done.35) | copy-start | bytes 589828
  300.5 84.4 %copy-start.58 = (pred[64,64]{1,0:T(8,128)(4,1)}, pred[64,64]{1,0:T(8,128)(4,1)S(1)}, u32[]{:S(2)}) copy-start(pred[64,64]{1,0:T(8,128)(4,1)S(1)} %iota_compare_fusion.2) | copy-start | bytes 12292
  308.2 72.5 %copy-start.54 = (f32[3,8,32]{2,1,0:T(8,128)}, f32[3,8,32]{2,1,0:T(8,128)S(1)}, u32[]{:S(2)}) copy-start(f32[3,8,32]{2,1,0:T(8,128)S(1)} %get-tuple-element.648) | copy-start | bytes 9220
  308.2 74.2 %copy-start.50 = (f32[3,8,32]{2,1,0:T(8,128)}, f32[3,8,32]{2,1,0:T(8,128)S(1)}, u32[]{:S(2)}) copy-start(f32[3,8,32]{2,1,0:T(8,128)S(1)} %get-tuple-element.647) | copy-start | bytes 9220
  368.9 63.4 %all-to-all-start.2 = ((bf16[64,12,2048]{2,1,0:T(8,128)(2,1)}), bf16[64,12,2048]{2,1,0:T(8,128)(2,1)}, u32[]{:S(2)}, u32[]{:S(2)}) async-start(bf16[64,12,2048]{2,1,0:T(8,128)(2,1)} %reshape.579), calls=%async_computation.2 | async-start | bytes 8388608 | tf_op jit(solution)/shard_map/all_to_all | solution.py:281
  462.3 31.8 %copy-start.85 = (f32[8,32]{1,0:T(8,128)S(1)}, f32[8,32]{1,0:T(8,128)}, u32[]{:S(2)}) copy-start(f32[8,32]{1,0:T(8,128)} %get-tuple-element.691) | copy-start | bytes 3076
  462.3 31.8 %copy-start.86 = (f32[8,32]{1,0:T(8,128)S(1)}, f32[8,32]{1,0:T(8,128)}, u32[]{:S(2)}) copy-start(f32[8,32]{1,0:T(8,128)} %get-tuple-element.692) | copy-start | bytes 3076
  465.4 42.1 %copy-start.91 = (f32[8,32]{1,0:T(8,128)S(1)}, f32[8,32]{1,0:T(8,128)}, u32[]{:S(2)}) copy-start(f32[8,32]{1,0:T(8,128)} %get-tuple-element.618) | copy-start | bytes 3076
  465.4 42.1 %copy-start.92 = (f32[8,32]{1,0:T(8,128)S(1)}, f32[8,32]{1,0:T(8,128)}, u32[]{:S(2)}) copy-start(f32[8,32]{1,0:T(8,128)} %get-tuple-element.619) | copy-start | bytes 3076
  465.4 42.1 %copy-start.101 = (f32[8,32]{1,0:T(8,128)S(1)}, f32[8,32]{1,0:T(8,128)}, u32[]{:S(2)}) copy-start(f32[8,32]{1,0:T(8,128)} %get-tuple-element.685) | copy-start | bytes 3076
  465.4 42.1 %copy-start.102 = (f32[8,32]{1,0:T(8,128)S(1)}, f32[8,32]{1,0:T(8,128)}, u32[]{:S(2)}) copy-start(f32[8,32]{1,0:T(8,128)} %get-tuple-element.686) | copy-start | bytes 3076
  465.4 42.1 %copy-start.103 = (f32[8,32]{1,0:T(8,128)S(1)}, f32[8,32]{1,0:T(8,128)}, u32[]{:S(2)}) copy-start(f32[8,32]{1,0:T(8,128)} %get-tuple-element.687) | copy-start | bytes 3076
  465.4 42.1 %copy-start.104 = (f32[8,32]{1,0:T(8,128)S(1)}, f32[8,32]{1,0:T(8,128)}, u32[]{:S(2)}) copy-start(f32[8,32]{1,0:T(8,128)} %get-tuple-element.688) | copy-start | bytes 3076
  564.7 43.2 %copy-start.89 = (f32[8,32]{1,0:T(8,128)S(1)}, f32[8,32]{1,0:T(8,128)}, u32[]{:S(2)}) copy-start(f32[8,32]{1,0:T(8,128)} %get-tuple-element.620) | copy-start | bytes 3076
  564.8 43.2 %copy-start.90 = (f32[8,32]{1,0:T(8,128)S(1)}, f32[8,32]{1,0:T(8,128)}, u32[]{:S(2)}) copy-start(f32[8,32]{1,0:T(8,128)} %get-tuple-element.621) | copy-start | bytes 3076
  564.8 43.2 %copy-start.97 = (f32[8,32]{1,0:T(8,128)S(1)}, f32[8,32]{1,0:T(8,128)}, u32[]{:S(2)}) copy-start(f32[8,32]{1,0:T(8,128)} %get-tuple-element.694) | copy-start | bytes 3076
  564.8 43.2 %copy-start.98 = (f32[8,32]{1,0:T(8,128)S(1)}, f32[8,32]{1,0:T(8,128)}, u32[]{:S(2)}) copy-start(f32[8,32]{1,0:T(8,128)} %get-tuple-element.695) | copy-start | bytes 3076
  564.8 43.2 %copy-start.99 = (f32[8,32]{1,0:T(8,128)S(1)}, f32[8,32]{1,0:T(8,128)}, u32[]{:S(2)}) copy-start(f32[8,32]{1,0:T(8,128)} %get-tuple-element.696) | copy-start | bytes 3076
  564.8 43.2 %copy-start.100 = (f32[8,32]{1,0:T(8,128)S(1)}, f32[8,32]{1,0:T(8,128)}, u32[]{:S(2)}) copy-start(f32[8,32]{1,0:T(8,128)} %get-tuple-element.697) | copy-start | bytes 3076
  569.0 40.4 %copy-start.57 = (f32[3,8,32]{2,1,0:T(8,128)S(1)}, f32[3,8,32]{2,1,0:T(8,128)}, u32[]{:S(2)}) copy-start(f32[3,8,32]{2,1,0:T(8,128)} %fusion.153) | copy-start | bytes 9220
  609.4 34.6 %copy-start.14 = (f32[3,64,8,32]{1,0,3,2:T(4,128)S(1)}, f32[3,64,8,32]{1,0,3,2:T(4,128)}, u32[]{:S(2)}) copy-start(f32[3,64,8,32]{1,0,3,2:T(4,128)} %mul.1406) | copy-start | bytes 589828
  609.4 37.1 %copy-start.87 = (f32[8,32]{1,0:T(8,128)S(1)}, f32[8,32]{1,0:T(8,128)}, u32[]{:S(2)}) copy-start(f32[8,32]{1,0:T(8,128)} %get-tuple-element.614) | copy-start | bytes 3076
  609.5 37.1 %copy-start.88 = (f32[8,32]{1,0:T(8,128)S(1)}, f32[8,32]{1,0:T(8,128)}, u32[]{:S(2)}) copy-start(f32[8,32]{1,0:T(8,128)} %get-tuple-element.615) | copy-start | bytes 3076
  609.5 37.1 %copy-start.93 = (f32[8,32]{1,0:T(8,128)S(1)}, f32[8,32]{1,0:T(8,128)}, u32[]{:S(2)}) copy-start(f32[8,32]{1,0:T(8,128)} %get-tuple-element.651) | copy-start | bytes 3076
  609.5 37.1 %copy-start.94 = (f32[8,32]{1,0:T(8,128)S(1)}, f32[8,32]{1,0:T(8,128)}, u32[]{:S(2)}) copy-start(f32[8,32]{1,0:T(8,128)} %get-tuple-element.652) | copy-start | bytes 3076
  609.5 37.1 %copy-start.95 = (f32[8,32]{1,0:T(8,128)S(1)}, f32[8,32]{1,0:T(8,128)}, u32[]{:S(2)}) copy-start(f32[8,32]{1,0:T(8,128)} %get-tuple-element.653) | copy-start | bytes 3076
  609.5 37.1 %copy-start.96 = (f32[8,32]{1,0:T(8,128)S(1)}, f32[8,32]{1,0:T(8,128)}, u32[]{:S(2)}) copy-start(f32[8,32]{1,0:T(8,128)} %get-tuple-element.654) | copy-start | bytes 3076
  670.1 65.5 %all-to-all-start.3 = ((f32[64,32,512]{2,1,0:T(8,128)}), f32[64,32,512]{2,1,0:T(8,128)}, u32[]{:S(2)}, u32[]{:S(2)}) async-start(f32[64,32,512]{2,1,0:T(8,128)} %bitcast.750), calls=%async_computation.3 | async-start | bytes 8388608 | tf_op jit(solution)/shard_map/all_to_all | solution.py:61
  (79 other events, 970.7 us)
where the time goes:
time: 749 us; the launch traced here: 739 us
  blocking collectives  289 us (39%)
  local copies, waits for them, and re-layouts  158 us (21%)
  other arithmetic  136 us (18%)
  matrix products  89.9 us (12%)
  waiting for transfers between devices  33 us (4%)
  starting transfers between devices  29.9 us (4%)
    all_gather x22, blocking collectives, prefix_by_axis(): pieces = jax.tree.map(lambda part: lax.all_gather(part, axis), so_far)  279 us
    another operation x8, other arithmetic  37.4 us
    all_to_all x1, waiting for transfers between devices, local(): lax.all_to_all(summed.reshape(cot_in.shape[0], cot_in.shape[1], summed.sh...  33 us
    another operation x4, other arithmetic, decayed_pass(): jnp.cumsum(log_rate.reshape(blocks, BLK, head_count, key_width), axis=1)  25.3 us
    unnamed x238, local copies, waits for them, and re-layouts  16.9 us
  transfers between devices with their start and end apart: 3, of which 1 were waited for; matrix products, arithmetic and copies ran while one was open for 24% of the time, Pallas kernels for 0%

commit v1 on v0

v1 whole, which is shorter than its diff:
```python
import functools

import jax
import jax.numpy as jnp
import numpy as np
from jax import lax
from jax.experimental import pallas as pl
from jax.experimental.pallas import tpu as pltpu
from jax.sharding import PartitionSpec as P

MESH = pl.DeviceIdType.MESH
BF = jnp.bfloat16
F32 = jnp.float32
NSP = 64
CAP = 12
TOK = 192
D = 2048
HD = 1024
FL = 512
NT = (((1,), (1,)), ((), ()))
TN = (((0,), (0,)), ((), ()))
NN = (((1,), (0,)), ((), ()))
ANY = pl.BlockSpec(memory_space=pl.ANY)
VM = pl.BlockSpec(memory_space=pltpu.VMEM)


def mm(a, b, dims=NN):
    return lax.dot_general(a, b, dims, preferred_element_type=F32)


def comps(k):
    return (k // 16, (k // 4) % 4, k % 4)


def shifted(me, off):
    z, y, x = me // 16, (me // 4) % 4, me % 4
    dz, dy, dx = off
    return ((z + dz) % 4) * 16 + ((y + dy) % 4) * 4 + (x + dx) % 4


def neg(k):
    a, b, c = comps(k)
    return ((-a) % 4) * 16 + ((-b) % 4) * 4 + (-c) % 4


def turned(k):
    a, b, c = comps(k)
    return b * 16 + c * 4 + a


def send_order():
    far = sorted(range(1, NSP), key=lambda k: -sum(min(a, 4 - a) for a in comps(k)))
    out = []
    for k in far:
        k2, k3 = turned(k), turned(turned(k))
        for q in (k, neg(k), k2, neg(k2), k3, neg(k3)):
            if q not in out:
                out.append(q)
    return out


ORDER = send_order()


def announce(sp, tp, barrier):
    def signal(k, c):
        pl.semaphore_signal(
            barrier, inc=1, device_id={"sp": shifted(sp, comps(k))}, device_id_type=MESH
        )
        return c

    lax.fori_loop(1, NSP, signal, 0)
    pl.semaphore_signal(barrier, inc=1, device_id={"tp": 1 - tp}, device_id_type=MESH)


def slot_codes(ids, bound):
    expert = lax.broadcasted_iota(jnp.int32, (NSP, TOK), 0).astype(F32)
    before = (
        lax.broadcasted_iota(jnp.int32, (TOK, TOK), 0)
        < lax.broadcasted_iota(jnp.int32, (TOK, TOK), 1)
    ).astype(F32).astype(BF)
    o0 = (expert == ids[0:1]).astype(F32)
    o1 = (expert == ids[1:2]).astype(F32)
    r0 = jnp.sum(o0 * mm(o0.astype(BF), before), axis=0, keepdims=True)
    c0 = jnp.sum(o0, axis=1, keepdims=True)
    r1 = jnp.sum(o1 * (mm(o1.astype(BF), before) + c0), axis=0, keepdims=True)
    return ids[0:1] * bound + r0, ids[1:2] * bound + r1


def expert_kernel(
    ids_ref, gates_ref, code_ref, back_ref, cot_hbm, mix_hbm, wg_hbm, wu_hbm, wd_hbm,
    c_out, t_out, h_out, g_out, u_out, mid_out,
    cot, mix, wg, wu, wd, xs, ra, rb, co, ct, to, tt, hid, gpg, upg, pown, poth, pin, ret, rr, mid, midp,
    ld, ssem, rsem, fs, fr, ps, pr, bs, br, ms, mr, od,
):
    sp, tp = lax.axis_index("sp"), lax.axis_index("tp")
    mine = pl.ds(pl.multiple_of(tp * HD, HD), HD)
    other = pl.ds(pl.multiple_of((1 - tp) * HD, HD), HD)
    loads = [
        pltpu.make_async_copy(cot_hbm.at[:, mine], cot, ld.at[0]),
        pltpu.make_async_copy(mix_hbm.at[:, mine], mix, ld.at[1]),
        pltpu.make_async_copy(wg_hbm, wg, ld.at[2]),
        pltpu.make_async_copy(wu_hbm, wu, ld.at[3]),
        pltpu.make_async_copy(wd_hbm, wd, ld.at[4]),
    ]
    for c in loads:
        c.start()
    barrier = pltpu.get_barrier_semaphore()
    announce(sp, tp, barrier)
    ids = ids_ref[...].astype(F32)
    d0, d1 = slot_codes(ids, float(CAP))
    g0, g1 = gates_ref[0:1], gates_ref[1:2]
    loads[0].wait()
    loads[1].wait()

    def pack(i, c):
        code = code_ref[pl.ds(i * 192, 192), :]
        cc, tc = code[:, 0:1], code[:, 1:2]
        m0, m1 = cc == d0, cc == d1
        selc = (m0 | m1).astype(F32).astype(BF)
        selt = ((tc == d0) | (tc == d1)).astype(F32).astype(BF)
        gate = jnp.sum(jnp.where(m0, g0, 0.0) + jnp.where(m1, g1, 0.0), axis=1, keepdims=True)
        gate = gate + (tc >= 0.0).astype(F32)
        rows = (mm(selc, cot[...]) + mm(selt, mix[...])) * gate
        xs[pl.ds(i * 24, 24)] = rows.reshape(24, 8, HD).astype(BF)
        return c

    lax.fori_loop(0, 8, pack, 0)
    pl.semaphore_wait(barrier, NSP)

    def out_copy(k):
        d = shifted(sp, comps(k))
        return pltpu.make_async_remote_copy(
            src_ref=xs.at[pl.ds(3 * d, 3)], dst_ref=ra.at[pl.ds(3 * sp, 3)],
            send_sem=ssem.at[k], recv_sem=rsem.at[k],
            device_id={"sp": d}, device_id_type=MESH,
        )

    def pass_copy(k):
        s = shifted(sp, comps(neg(k)))
        return pltpu.make_async_remote_copy(
            src_ref=ra.at[pl.ds(3 * s, 3)], dst_ref=rb.at[pl.ds(3 * s, 3)],
            send_sem=fs.at[k], recv_sem=fr.at[k],
            device_id={"tp": 1 - tp}, device_id_type=MESH,
        )

    for k in ORDER:
        out_copy(k).start()
    ra[pl.ds(3 * sp, 3)] = xs[pl.ds(3 * sp, 3)]
    pass_copy(0).start()
    for k in ORDER:
        out_copy(k).wait_recv()
        pass_copy(k).start()
    loads[2].wait()
    loads[3].wait()
    loads[4].wait()
    for k in [0] + ORDER:
        pass_copy(k).wait_recv()

    def split(buf, i, cdst, tdst):
        x = buf[pl.ds(i * 48, 48)].astype(F32).reshape(8, 6, 8, HD)
        a, b = x[:, 2], x[:, 5]
        cm = jnp.concatenate([a[:, 0:4], b[:, 0:4]], axis=1)
        tm = jnp.concatenate([a[:, 4:8], b[:, 4:8]], axis=1)
        cv = jnp.stack([x[:, 0], x[:, 3], cm], axis=1).reshape(192, HD)
        tv = jnp.stack([x[:, 1], x[:, 4], tm], axis=1).reshape(192, HD)
        cdst[pl.ds(i * 192, 192), :] = cv.astype(BF)
        tdst[pl.ds(i * 192, 192), :] = tv.astype(BF)

    def parts(i, c):
        split(ra, i, co, to)
        split(rb, i, ct, tt)
        return c

    lax.fori_loop(0, 4, parts, 0)
    outs = [
        pltpu.make_async_copy(co, c_out.at[:, mine], od.at[0]),
        pltpu.make_async_copy(ct, c_out.at[:, other], od.at[1]),
        pltpu.make_async_copy(to, t_out.at[:, mine], od.at[2]),
        pltpu.make_async_copy(tt, t_out.at[:, other], od.at[3]),
    ]
    for c in outs:
        c.start()

    def chunk(i, c):
        rows = pl.ds(i * 384, 384)
        t1, t2, c1, c2 = to[rows, :], tt[rows, :], co[rows, :], ct[rows, :]
        gate_pre = mm(t1, wg[mine, :]) + mm(t2, wg[other, :])
        up_pre = mm(t1, wu[mine, :]) + mm(t2, wu[other, :])
        hidden_grad = mm(c1, wd[:, mine], NT) + mm(c2, wd[:, other], NT)
        sg = jax.nn.sigmoid(gate_pre)
        silu = gate_pre * sg
        hid[rows, :] = (silu * up_pre).astype(BF)
        slope = sg * (1.0 + gate_pre * (1.0 - sg))
        gg = (hidden_grad * up_pre * slope).astype(BF)
        ug = (hidden_grad * silu).astype(BF)
        gpg[rows, :] = gg
        upg[rows, :] = ug
        poth[rows, :] = (mm(gg, wg[other, :], NT) + mm(ug, wu[other, :], NT)).astype(BF)
        pown[rows, :] = (mm(gg, wg[mine, :], NT) + mm(ug, wu[mine, :], NT)).astype(BF)
        return c

    lax.fori_loop(0, 2, chunk, 0)
    outs2 = [
        pltpu.make_async_copy(hid, h_out, od.at[4]),
        pltpu.make_async_copy(gpg, g_out, od.at[5]),
        pltpu.make_async_copy(upg, u_out, od.at[6]),
    ]
    for c in outs2:
        c.start()
    swap = pltpu.make_async_remote_copy(
        src_ref=poth, dst_ref=pin, send_sem=ps, recv_sem=pr,
        device_id={"tp": 1 - tp}, device_id_type=MESH,
    )
    swap.start()
    swap.wait_recv()

    def sums(i, c):
        rows = pl.ds(i * 192, 192)
        v = (pown[rows, :].astype(F32) + pin[rows, :].astype(F32)).reshape(8, 3, 8, HD)
        m = v[:, 2]
        e = jnp.concatenate([m[:, 0:4, 0:512], m[:, 0:4, 512:1024]], axis=1)
        o = jnp.concatenate([m[:, 4:8, 0:512], m[:, 4:8, 512:1024]], axis=1)
        ev = jnp.concatenate([v[:, 0], e], axis=2)
        ov = jnp.concatenate([v[:, 1], o], axis=2)
        ret[pl.ds(i * 16, 16)] = jnp.stack([ev, ov], axis=1).reshape(16, 8, 1536).astype(BF)
        return c

    lax.fori_loop(0, 4, sums, 0)

    def back_copy(k):
        d = shifted(sp, comps(k))
        return pltpu.make_async_remote_copy(
            src_ref=ret.at[d], dst_ref=rr.at[sp],
            send_sem=bs.at[k], recv_sem=br.at[k],
            device_id={"sp": d}, device_id_type=MESH,
        )

    for k in ORDER:
        back_copy(k).start()
    rr[sp] = ret[sp]
    bc = back_ref[...]
    e0 = ((bc[:, 0:1] == d0) | (bc[:, 0:1] == d1)).astype(F32).astype(BF)
    e1 = ((bc[:, 1:2] == d0) | (bc[:, 1:2] == d1)).astype(F32).astype(BF)
    e2 = ((bc[:, 2:3] == d0) | (bc[:, 2:3] == d1)).astype(F32).astype(BF)
    for k in ORDER:
        back_copy(k).wait_recv()
    full = rr[...].reshape(512, 1536)
    late = full[:, 1024:1536]
    acc = mm(e0, full[:, 0:1024], TN)
    lo, hi = mm(e1, late, TN), mm(e2, late, TN)
    mid[...] = (cot[...].astype(F32) + acc + jnp.concatenate([lo, hi], axis=1)).astype(BF)
    give = pltpu.make_async_remote_copy(
        src_ref=mid, dst_ref=midp, send_sem=ms, recv_sem=mr,
        device_id={"tp": 1 - tp}, device_id_type=MESH,
    )
    give.start()
    m1 = pltpu.make_async_copy(mid, mid_out.at[:, mine], od.at[7])
    m1.start()
    give.wait_recv()
    m2 = pltpu.make_async_copy(midp, mid_out.at[:, other], od.at[8])
    m2.start()
    for k in ORDER:
        out_copy(k).wait_send()
        pass_copy(k).wait_send()
        back_copy(k).wait_send()
    pass_copy(0).wait_send()
    swap.wait_send()
    give.wait_send()
    for c in outs + outs2 + [m1, m2]:
        c.wait()


def row_codes():
    code = np.full((NSP, 24, 2), -1.0, np.float32)
    back = np.full((NSP, 8, 3), -1.0, np.float32)
    for e in range(NSP):
        for u in range(8):
            code[e, u, 0] = code[e, 8 + u, 1] = e * CAP + u
            back[e, u, 0] = e * CAP + u
        for u in range(4):
            code[e, 16 + u, 0] = code[e, 20 + u, 1] = e * CAP + 8 + u
            back[e, u, 1] = back[e, 4 + u, 2] = e * CAP + 8 + u
    return code.reshape(NSP * 24, 2), back.reshape(NSP * 8, 3)


def experts(cotangent, mixed_input, route_ids, route_gates, wg, wu, wd):
    code, back = row_codes()
    dma = pltpu.SemaphoreType.DMA
    v = lambda *s: pltpu.VMEM(s, BF)
    rows = NSP * CAP
    out = lambda *s: jax.ShapeDtypeStruct(s, BF)
    return pl.pallas_call(
        expert_kernel,
        out_shape=(
            out(rows, D), out(rows, D), out(rows, FL), out(rows, FL), out(rows, FL), out(TOK, D),
        ),
        in_specs=[VM, VM, VM, VM, ANY, ANY, ANY, ANY, ANY],
        out_specs=(ANY,) * 6,
        scratch_shapes=[
            v(TOK, HD), v(TOK, HD), v(D, FL), v(D, FL), v(FL, D),
            v(192, 8, HD), v(192, 8, HD), v(192, 8, HD),
            v(rows, HD), v(rows, HD), v(rows, HD), v(rows, HD),
            v(rows, FL), v(rows, FL), v(rows, FL),
            v(rows, HD), v(rows, HD), v(rows, HD),
            v(NSP, 8, 1536), v(NSP, 8, 1536), v(TOK, HD), v(TOK, HD),
            dma((5,)), dma((NSP,)), dma((NSP,)), dma((NSP,)), dma((NSP,)), dma, dma,
            dma((NSP,)), dma((NSP,)), dma, dma, dma((9,)),
        ],
        compiler_params=pltpu.CompilerParams(
            collective_id=1, has_side_effects=True, vmem_limit_bytes=60 * 1024 * 1024
        ),
        name="experts",
    )(
        route_ids.T, route_gates.T, jnp.asarray(code), jnp.asarray(back),
        cotangent, mixed_input, wg, wu, wd,
    )


def halves(x):
    hi = x.astype(BF)
    return hi, (x - hi.astype(F32)).astype(BF)


def exact_left(ones, x, dims=NN):
    hi, lo = halves(x)
    rest = (x - hi.astype(F32) - lo.astype(F32)).astype(BF)
    return mm(ones, hi, dims) + mm(ones, lo, dims) + mm(ones, rest, dims)


def left2(x, b, dims):
    hi, lo = halves(x)
    return mm(hi, b, dims) + mm(lo, b, dims)


def right2(a, x, dims):
    hi, lo = halves(x)
    return mm(a, hi, dims) + mm(a, lo, dims)


def both3(a, b, dims):
    ah, al = halves(a)
    bh, bl = halves(b)
    return mm(ah, bh, dims) + mm(al, bh, dims) + mm(ah, bl, dims)


def iota(shape, dim):
    return lax.broadcasted_iota(jnp.int32, shape, dim)


def squeezed(top_of, low):
    return jnp.concatenate(
        [jnp.where(low, top_of(p)[0:32], top_of(p)[32:64]) for p in range(4)], axis=0
    )


def spread(comp, low):
    rows = []
    for p in range(4):
        c = comp[32 * p : 32 * p + 32]
        blk = jnp.concatenate([jnp.where(low, c, 0.0), jnp.where(low, 0.0, c)], axis=0)
        z = jnp.zeros((64, 128), F32)
        rows.append(jnp.concatenate([blk if j == p else z for j in range(4)], axis=1))
    return jnp.concatenate(rows, axis=0)


def mixer_kernel(
    mid_ref, proj_ref, mo_ref, q_ref, k_ref, v_ref, lf_ref, lb_ref,
    pg_out, q_out, k_out, v_out, f_out, b_out,
    g_s, pp, pin, st, sr, res, fin, qh, ql, kh, kl, dq_s, dk_s,
    ss, rs, s2, r2, s3, r3,
):
    sp, tp = lax.axis_index("sp"), lax.axis_index("tp")
    barrier = pltpu.get_barrier_semaphore()
    announce(sp, tp, barrier)
    scale = 32.0 ** -0.5
    rows_i, cols_i = iota((TOK, TOK), 0), iota((TOK, TOK), 1)
    lower = (cols_i <= rows_i).astype(F32).astype(BF)
    upper = (cols_i >= rows_i).astype(F32).astype(BF)
    lf, lb = lf_ref[...], lb_ref[...]
    pf, pb = exact_left(lower, lf), exact_left(upper, lb)
    tf, tb = pf[TOK - 1 : TOK], pb[0:1]
    cf, cb = pf[95:96], pb[96:97]
    qs = q_ref[...].astype(F32) * scale
    kv = k_ref[...].astype(F32)
    vals = v_ref[...]
    mix = mm(mid_ref[...], proj_ref[...]).astype(BF)
    g_s[...] = mix
    low = iota((32, 128), 1) < 64
    ones = jnp.ones((TOK, 128), BF)

    def wide(x, y):
        w = left2(x, y, TN)
        return squeezed(lambda p: w[64 * p : 64 * p + 64, 128 * p : 128 * p + 128], low)

    def decays(x):
        hi, lo = halves(x)
        rest = (x - hi.astype(F32) - lo.astype(F32)).astype(BF)
        w = jnp.exp(mm(hi, ones, TN) + mm(lo, ones, TN) + mm(rest, ones, TN))
        return squeezed(lambda p: w[64 * p : 64 * p + 64], low)

    kef, keb = kv * jnp.exp(tf - pf), kv * jnp.exp(tb - pb)
    df, db = decays(lf), decays(lb)
    maps = (
        wide(kef, vals), wide(keb, vals), wide(qs * jnp.exp(pf), mix), wide(qs * jnp.exp(pb), mix),
        df, db, df, db,
    )
    for j, m in enumerate(maps):
        for i in range(2):
            st[pl.ds(2 * j + i, NSP, stride=16), :] = m[64 * i : 64 * i + 64]
    pl.semaphore_wait(barrier, NSP)

    def state_copy(k):
        d = shifted(sp, comps(k))
        return pltpu.make_async_remote_copy(
            src_ref=st.at[pl.ds(pl.multiple_of(16 * d, 16), 16)],
            dst_ref=sr.at[pl.ds(pl.multiple_of(16 * sp, 16), 16)],
            send_sem=ss.at[k], recv_sem=rs.at[k], device_id={"sp": d}, device_id_type=MESH,
        )

    def result_copy(k):
        d = shifted(sp, comps(k))
        return pltpu.make_async_remote_copy(
            src_ref=res.at[pl.ds(pl.multiple_of(8 * d, 8), 8)],
            dst_ref=fin.at[pl.ds(pl.multiple_of(8 * sp, 8), 8)],
            send_sem=s2.at[k], recv_sem=r2.at[k], device_id={"sp": d}, device_id_type=MESH,
        )

    def proj_copy(k):
        d = shifted(sp, comps(k))
        return pltpu.make_async_remote_copy(
            src_ref=pp.at[d], dst_ref=pin.at[sp],
            send_sem=s3.at[k], recv_sem=r3.at[k], device_id={"sp": d}, device_id_type=MESH,
        )

    for k in ORDER:
        state_copy(k).start()
    own16 = pl.ds(pl.multiple_of(16 * sp, 16), 16)
    sr[own16, :] = st[own16, :]

    def part(i, c):
        cols = pl.ds(pl.multiple_of(i * 512, 512), 512)
        pp[pl.ds(16 * i, 16)] = mm(mid_ref[:, cols], mo_ref[...], TN).reshape(16, 32, FL).astype(BF)
        return c

    lax.fori_loop(0, 4, part, 0)
    for n, (p, c) in enumerate(((pf, cf), (pb, cb))):
        qh[n], ql[n] = halves(qs * jnp.exp(p - c))
        kh[n], kl[n] = halves(kv * jnp.exp(c - p))
    dq_s[...] = jnp.zeros_like(dq_s)
    dk_s[...] = jnp.zeros_like(dk_s)
    v_out[...] = jnp.zeros_like(v_out)
    lane = iota((TOK, 128), 1)

    def head(h, carry):
        pair = pl.ds(pl.multiple_of((h // 2) * 128, 128), 128)
        tile = pl.ds(pl.multiple_of((h // 4) * 128, 128), 128)
        half = (lane // 64) == h % 2
        quarter = (lane // 32) == h % 4
        gp, vp = g_s[:, pair], v_ref[:, pair]
        gh = jnp.where(half, gp, jnp.zeros_like(gp))
        da = mm(gh, vp, NT)
        dat = mm(vp, gh, NT)
        at = jnp.zeros((TOK, TOK), F32)
        for n in range(2):
            keep = cols_i <= rows_i if n == 0 else cols_i >= rows_i
            keep_t = cols_i >= rows_i if n == 0 else cols_i <= rows_i
            pick = lambda r: jnp.where(quarter, r[n, :, tile], jnp.zeros((TOK, 128), BF))
            a, b, c, d = pick(qh), pick(ql), pick(kh), pick(kl)
            s = mm(c, a, NT) + mm(c, b, NT) + mm(d, a, NT)
            at = at + jnp.where(keep_t, s, 0.0)
            hi, lo = halves(jnp.where(keep, da, 0.0))
            dq_s[n, :, tile] += mm(hi, c) + mm(hi, d) + mm(lo, c)
            hi, lo = halves(jnp.where(keep_t, dat, 0.0))
            dk_s[n, :, tile] += mm(hi, a) + mm(hi, b) + mm(lo, a)
        v_out[:, pair] += left2(at, gh, NN)
        return carry

    lax.fori_loop(0, 4, head, 0)
    for k in ORDER:
        state_copy(k).wait_recv()

    def up(s, u):
        at = pl.multiple_of(16 * s, 16)
        res[pl.ds(pl.multiple_of(8 * s, 8), 8), :] = u
        return sr[pl.ds(at + 8, 8), :] * u + sr[pl.ds(at, 8), :]

    r8 = iota((8, 128), 0)
    rising = (r8 < 2) | (r8 >= 6)

    def down(i, w):
        s = NSP - 1 - i
        at, to = pl.multiple_of(16 * s, 16), pl.ds(pl.multiple_of(8 * s, 8), 8)
        res[to, :] = jnp.where(rising, res[to, :], w)
        return sr[pl.ds(at + 8, 8), :] * w + sr[pl.ds(at, 8), :]

    zero = jnp.zeros((8, 128), F32)
    lax.fori_loop(0, NSP, up, zero)
    lax.fori_loop(0, NSP, down, zero)
    for k in ORDER:
        result_copy(k).start()
    own8 = pl.ds(pl.multiple_of(8 * sp, 8), 8)
    fin[own8, :] = res[own8, :]
    for k in ORDER:
        proj_copy(k).start()
    pin[sp] = pp[sp]
    lax.fori_loop(4, 8, head, 0)
    for k in ORDER:
        result_copy(k).wait_recv()

    def found(j):
        return spread(
            jnp.concatenate([fin[pl.ds(2 * j + i, NSP, stride=8), :] for i in range(2)], axis=0), low
        )

    sf, sb, gf, gb = found(0), found(1), found(2), found(3)
    ones8 = jnp.ones((8, FL), BF)
    dqs, dks = 0.0, 0.0
    for n, (p, c, t, ke, s, g, sums, out) in enumerate(
        ((pf, cf, tf, kef, sf, gf, upper, f_out), (pb, cb, tb, keb, sb, gb, lower, b_out))
    ):
        dq = jnp.exp(p - c) * dq_s[n] + jnp.exp(p) * right2(mix, s, NT)
        ik = jnp.exp(t - p) * right2(vals, g, NT)
        dk = jnp.exp(c - p) * dk_s[n] + ik
        both = exact_left(ones8, s * g, NT)[0:1]
        total = jnp.exp(t) * both + jnp.sum(kv * ik, axis=0, keepdims=True)
        out[...] = exact_left(sums, qs * dq - kv * dk) + total
        v_out[...] += both3(ke, g, NN)
        dqs, dks = dqs + dq, dks + dk
    q_out[...] = dqs * scale
    k_out[...] = dks
    for k in ORDER:
        proj_copy(k).wait_recv()

    def add(i, acc):
        return acc + pin[i].astype(F32)

    pg_out[...] = lax.fori_loop(0, NSP, add, jnp.zeros((32, FL), F32))
    for k in ORDER:
        state_copy(k).wait_send()
        result_copy(k).wait_send()
        proj_copy(k).wait_send()


def mixer(mid, proj, mo, q, k, v, lf, lb):
    dma = pltpu.SemaphoreType.DMA
    f = lambda *s: jax.ShapeDtypeStruct(s, F32)
    vb = lambda *s: pltpu.VMEM(s, BF)
    vf = lambda *s: pltpu.VMEM(s, F32)
    return pl.pallas_call(
        mixer_kernel,
        out_shape=(f(32, FL), f(TOK, 256), f(TOK, 256), f(TOK, FL), f(TOK, 256), f(TOK, 256)),
        in_specs=[VM] * 8,
        out_specs=(VM,) * 6,
        scratch_shapes=[
            vb(TOK, FL), vb(NSP, 32, FL), vb(NSP, 32, FL), vf(1024, 128), vf(1024, 128),
            vf(512, 128), vf(512, 128), vb(2, TOK, 256), vb(2, TOK, 256), vb(2, TOK, 256),
            vb(2, TOK, 256), vf(2, TOK, 256), vf(2, TOK, 256),
        ]
        + [dma((NSP,))] * 6,
        compiler_params=pltpu.CompilerParams(
            collective_id=2, has_side_effects=True, vmem_limit_bytes=56 * 1024 * 1024
        ),
        name="mixer",
    )(mid, proj, mo, q, k, v, lf, lb)


def local(
    cotangent, mixed_input, route_ids, route_gates, expert_gate, expert_up, expert_down,
    projection, mixer_output, query_rows, key_rows, value_rows, log_forward, log_backward,
):
    c, t, h, gg, ug, mid = experts(
        cotangent, mixed_input, route_ids, route_gates, expert_gate[0], expert_up[0], expert_down[0]
    )
    rest = mixer(
        mid, projection, mixer_output, query_rows, key_rows, value_rows, log_forward, log_backward
    )
    return (mm(t, gg, TN)[None], mm(t, ug, TN)[None], mm(h, c, TN)[None], *rest)


def solution(mesh):
    sp, tok = P("sp", None), P("sp", "tp")
    ein, eout = P("sp", None, "tp"), P("sp", "tp", None)
    return jax.shard_map(
        local,
        mesh=mesh,
        in_specs=(sp, sp, sp, sp, ein, ein, eout, P(None, "tp")) + (tok,) * 6,
        out_specs=(ein, ein, eout) + (tok,) * 6,
        check_vma=False,
    )
```

time: 749 us -> 166 us (0.22); the launches traced: 739 us -> 165 us
  blocking collectives: 289 us -> 0 us
  local copies, waits for them, and re-layouts: 158 us -> 9.72 us
  Pallas kernels: 0 us -> 141 us
  other arithmetic: 136 us -> 0 us
  matrix products: 89.9 us -> 13.9 us
  waiting for transfers between devices: 33 us -> 0 us
  starting transfers between devices: 29.9 us -> 0 us
    all_gather x22 -> x0, blocking collectives: 279 us -> none  [prefix_by_axis(): pieces = jax.tree.map(lambda part: lax.all_gather(part, axis), so_far)]
    pallas_call x0 -> x2, Pallas kernels: none -> 141 us  [the longest x1 88.6 us: experts(): pl.pallas_call(expert_kernel, out_shape=(out(rows, D), out(rows, D), out(...]
    dot_general x34 -> x3, matrix products: 89.9 us -> 13.9 us  [mm(): return lax.dot_general(a, b, dims, preferred_element_type=F32)]
    another operation x12 -> x0, other arithmetic: 62.7 us -> none
    reshape x16 -> x0, local copies, waits for them, and re-layouts: 39.7 us -> none  [the longest x1 6.17 us: local(): cot_block = cot_in.reshape(row_total, feature_count)]
    all_to_all x3 -> x0, waiting for transfers between devices: 33 us -> none  [the longest x1 33 us: local(): lax.all_to_all(summed.reshape(cot_in.shape[0], cot_in.shape[1], summed.sh...]
    all_to_all x3 -> x0, starting transfers between devices: 29.9 us -> none  [the longest x1 12.4 us: sent_together(): lax.all_to_all(both, axis, split_axis=split_dim, concat_axis=concat_dim,...]
    reduce_sum x10 -> x0, other arithmetic: 22.6 us -> none  [the longest x1 6.89 us: of_everyone(): return from_everyone(x, axis).astype(jnp.float32).sum(axis=0)]
  transfers between devices with their start and end apart: 3 -> 0, of which waited for: 1 -> 0; matrix products, arithmetic and copies ran while one was open for 24% -> 0% of each run, Pallas kernels for 0% -> 0%
where the time goes in v1:
time: 166 us; the launch traced here: 165 us
  Pallas kernels  141 us (85%)
  matrix products  13.9 us (8%)
  local copies, waits for them, and re-layouts  9.72 us (6%)
    pallas_call x1, Pallas kernels, experts(): pl.pallas_call(expert_kernel, out_shape=(out(rows, D), out(rows, D), out(...  88.6 us
    pallas_call x1, Pallas kernels, mixer(): pl.pallas_call(mixer_kernel, out_shape=(f(32, FL), f(TOK, 256), f(TOK, 25...  52.4 us
    dot_general x3, matrix products, mm(): return lax.dot_general(a, b, dims, preferred_element_type=F32)  13.9 us
    unnamed x14, local copies, waits for them, and re-layouts  9.72 us

profile of v1, /device:TPU:0, one launch (start us, length us, event | category | flops | bytes accessed | tf_op | source)
XLA Modules:
  0.0 165.3 jit_solution(2926912536145110827)
XLA Ops:
  0.6 88.6 %experts.1 = (bf16[768,2048]{1,0:T(8,128)(2,1)}, bf16[768,2048]{1,0:T(8,128)(2,1)}, bf16[768,512]{1,0:T(8,128)(2,1)}, bf16[768,512]{1,0:T(8,128)(2,1)}, bf16[768...) custom-call(s32[2,192]{1,0:T(2,128)} %bitcast.20, f32[2,192]{1,0:T(2,128)} %bitcast.21, f32[1536,2]{1,0:T(8,128)} %constant.4.clone.code_ref, ...), custom_call_target="tpu_custom_call" | custom-call | tf_op jit(solution)/shard_map/experts/pallas_call | solution.py:293
  89.3 0.0 copy-start.2
  89.3 0.0 copy-start.3
  89.3 6.1 %convolution_bitcast_fusion.1 = f32[1,2048,512]{2,1,0:T(8,128)} fusion(bf16[768,2048]{1,0:T(8,128)(2,1)} %get-tuple-element.21, bf16[768,512]{1,0:T(8,128)(2,1)} %get-tuple-element.23), kind=kOutput, calls=%fused_computation.1 | convolution fusion | flops 1610612736 | bytes 8126464 | tf_op jit(solution)/shard_map/dot_general | solution.py:28
  95.4 0.0 copy-done.2
  95.4 0.0 copy-done.3
  95.4 0.0 copy-start
  95.4 0.0 copy-start.1
  95.4 3.9 %convolution_bitcast_fusion.2 = f32[1,2048,512]{2,1,0:T(8,128)} fusion(bf16[768,2048]{1,0:T(8,128)(2,1)S(1)} %copy-done.2, bf16[768,512]{1,0:T(8,128)(2,1)S(1)} %copy-done.3), kind=kOutput, calls=%fused_computation.2 | convolution fusion | flops 1610612736 | bytes 8126464 | tf_op jit(solution)/shard_map/dot_general | solution.py:28
  99.3 0.0 copy-done
  99.3 0.0 copy-done.1
  99.3 3.9 %convolution_bitcast_fusion = f32[1,512,2048]{2,1,0:T(8,128)} fusion(bf16[768,512]{1,0:T(8,128)(2,1)S(1)} %copy-done.1, bf16[768,2048]{1,0:T(8,128)(2,1)S(1)} %copy-done), kind=kOutput, calls=%fused_computation | convolution fusion | flops 1610612736 | bytes 8126464 | tf_op jit(solution)/shard_map/dot_general | solution.py:28
  103.2 52.4 %mixer.1 = (f32[32,512]{1,0:T(8,128)}, f32[192,256]{1,0:T(8,128)}, f32[192,256]{1,0:T(8,128)}, f32[192,512]{1,0:T(8,128)}, f32[192,256]{1,0:T(8,128)}, /*index=5*/f32[192,256]{1,0:T(8,128)}) custom-call(bf16[192,2048]{1,0:T(8,128)(2,1)} %get-tuple-element.26.mid_ref, bf16[2048,512]{1,0:T(8,128)(2,1)} %proj_ref.1, bf16[192,512]{1,0:T(8,128)(2,1)} %mo_ref.1, ...), custom_call_target="tpu_custom_call" | custom-call | tf_op jit(solution)/shard_map/mixer/pallas_call | solution.py:550
  155.6 1.5 copy.31
  157.1 1.6 copy.32
  158.7 1.6 copy.33
  160.3 1.8 %copy.34 = f32[192,512]{1,0:T(8,128)} copy(f32[192,512]{1,0:T(8,128)} %get-tuple-element.48) | data formatting | bytes 786432
  162.0 1.6 copy.35
  163.7 1.6 copy.36
Async XLA Ops:
  89.3 6.1 %copy-start.2 = (bf16[768,2048]{1,0:T(8,128)(2,1)S(1)}, bf16[768,2048]{1,0:T(8,128)(2,1)}, u32[]{:S(2)}) copy-start(bf16[768,2048]{1,0:T(8,128)(2,1)} %get-tuple-element.21) | copy-start | bytes 9437188
  89.3 6.1 %copy-start.3 = (bf16[768,512]{1,0:T(8,128)(2,1)S(1)}, bf16[768,512]{1,0:T(8,128)(2,1)}, u32[]{:S(2)}) copy-start(bf16[768,512]{1,0:T(8,128)(2,1)} %get-tuple-element.22) | copy-start | bytes 2359300
  95.4 3.9 %copy-start = (bf16[768,2048]{1,0:T(8,128)(2,1)S(1)}, bf16[768,2048]{1,0:T(8,128)(2,1)}, u32[]{:S(2)}) copy-start(bf16[768,2048]{1,0:T(8,128)(2,1)} %get-tuple-element.25) | copy-start | bytes 9437188
  95.4 3.9 %copy-start.1 = (bf16[768,512]{1,0:T(8,128)(2,1)S(1)}, bf16[768,512]{1,0:T(8,128)(2,1)}, u32[]{:S(2)}) copy-start(bf16[768,512]{1,0:T(8,128)(2,1)} %get-tuple-element.24) | copy-start | bytes 2359300
